TPU v7x, 1024 devices: a whole 8x8x8 slice. The times are simulated.
1024 devices in a mesh: ep: 64 (over z, y), tp: 16 (over x, core).
Axes of the slice: x: 8, y: 8, z: 8, core: 2. Of those that a mesh axis runs over, the one named last changes fastest.
Arguments:
- tokens: bfloat16 [8192, 2048], P('ep'), may hold values from -36 to 36, as said below
- norm_gain: float32 [2048], replicated, may hold values from 0.1 to 1.9
- chosen: int32 [8, 2048], replicated, may hold values from 0 to 8191, as said below
- slot_weight: float32 [8, 2048], replicated, may hold values from 0.1 to 1
- gate_weight: bfloat16 [8, 2048, 4096], P(None, 'ep', 'tp'), may hold values from -0.125 to 0.125
- up_weight: bfloat16 [8, 2048, 4096], P(None, 'ep', 'tp'), may hold values from -0.125 to 0.125
- down_weight: bfloat16 [8, 2048, 4096], P(None, 'ep', 'tp'), may hold values from -0.09375 to 0.09375
Outputs:
- mixed: bfloat16 [8192, 2048], P('ep', 'tp')
Inputs may be any that keep to these rules, and one draw needn't show every extreme that they name: `tokens`: each entry is the scaled entry of a bounded draw; rows and features differ in scale. `chosen`: the 2048 slots of an expert name distinct tokens. Slots of an expert fall into aligned blocks of 256; within a block the token numbers ascend, and at most 8 of them lie among the 128 tokens of one index of ep (tokens i * 128 onward belong to index i); in every block some index supplies exactly 8.
All inputs are finite; a program needn't handle non-finite values.
Results may differ from a plain program's by a relative error of at most 0.019.
Values may be sent and summed in bfloat16 or wider, within the bound.
A program may use at most 32 MiB of HBM per device.

v0:
```python
import jax
import jax.numpy as jnp
from jax import lax
from jax.sharding import PartitionSpec as P

EPSILON = 1e-06


def cut_along(array, dim, peers):
    before, after = (array.shape[:dim], array.shape[dim + 1 :])
    return jnp.moveaxis(array.reshape(*before, peers, -1, *after), dim, 0)


def sum_at_owner(array, axis, dim):
    tiles = cut_along(array, dim, lax.axis_size(axis))
    arrived = lax.all_to_all(tiles, axis, split_axis=0, concat_axis=0, tiled=True)
    return arrived.astype(jnp.float32).sum(axis=0)


def body(tokens, norm_gain, chosen, slot_weight, gate_weight, up_weight, down_weight):
    expert_devices = lax.axis_size("ep")
    width_devices = lax.axis_size("tp")
    device_index = lax.axis_index("ep")
    local_tokens = tokens.shape[0]
    model_width = tokens.shape[1]
    expert_total = chosen.shape[0]
    group_size = expert_devices // expert_total
    slots_piece = chosen.shape[1] // group_size
    seat_count = 4 * local_tokens // expert_devices
    buffer_rows = expert_devices * seat_count
    column_width = model_width // width_devices
    values = tokens.astype(jnp.float32)
    scaled = values * lax.rsqrt(jnp.mean(values * values, axis=1, keepdims=True) + EPSILON)
    normed = (scaled * norm_gain).astype(jnp.bfloat16)
    piece_tokens = chosen.reshape(expert_devices, slots_piece)
    piece_weights = slot_weight.reshape(expert_devices, slots_piece)
    owners = piece_tokens // local_tokens
    is_mine = owners == device_index
    earlier = jnp.sum((owners < device_index).astype(jnp.int32), axis=1, keepdims=True)
    seat_index = jnp.arange(slots_piece, dtype=jnp.int32)[None, :] - earlier
    local_index = piece_tokens - device_index * local_tokens
    seat_range = jnp.arange(seat_count, dtype=jnp.int32)
    matches = is_mine[:, None, :] & (seat_index[:, None, :] == seat_range[None, :, None])
    filled = jnp.any(matches, axis=2).reshape(buffer_rows)
    source_index = jnp.sum(jnp.where(matches, local_index[:, None, :], 0), axis=2).reshape(
        buffer_rows
    )
    seat_weight = jnp.sum(jnp.where(matches, piece_weights[:, None, :], 0.0), axis=2).reshape(
        buffer_rows
    )
    my_tokens = lax.dynamic_index_in_dim(piece_tokens, device_index, 0, keepdims=False)
    my_owners = my_tokens // local_tokens
    before = jnp.sum((my_owners[None, :] < my_owners[:, None]).astype(jnp.int32), axis=1)
    arrival_row = my_owners * seat_count + jnp.arange(slots_piece, dtype=jnp.int32) - before
    gate_send = jnp.repeat(gate_weight, group_size, axis=0)
    up_send = jnp.repeat(up_weight, group_size, axis=0)
    down_send = jnp.repeat(down_weight, group_size, axis=0)
    gate_full, up_full = (
        lax.all_to_all(gate_send, "ep", split_axis=0, concat_axis=1, tiled=True),
        lax.all_to_all(up_send, "ep", split_axis=0, concat_axis=1, tiled=True),
    )
    down_full = lax.all_to_all(down_send, "ep", split_axis=0, concat_axis=1, tiled=True)
    empty_value = jnp.zeros((), jnp.bfloat16)
    outgoing = jnp.where(filled[:, None], jnp.take(normed, source_index, axis=0), empty_value)
    arrived = lax.all_to_all(
        outgoing.reshape(expert_devices, seat_count, model_width),
        "ep",
        split_axis=0,
        concat_axis=0,
        tiled=True,
    )
    slot_rows = jnp.take(arrived.reshape(buffer_rows, model_width), arrival_row, axis=0)
    gate_part = jnp.dot(slot_rows, gate_full[0], preferred_element_type=jnp.float32)
    up_part = jnp.dot(slot_rows, up_full[0], preferred_element_type=jnp.float32)
    hidden = (jax.nn.silu(gate_part) * up_part).astype(jnp.bfloat16)
    down_rows = down_full[0]
    summed = sum_at_owner(
        jnp.einsum("df,bf->db", down_rows, hidden, preferred_element_type=jnp.float32).astype(
            jnp.bfloat16
        ),
        "tp",
        0,
    ).astype(jnp.bfloat16)
    buffer_range = jnp.arange(buffer_rows, dtype=jnp.int32)
    hits = arrival_row[None, :] == buffer_range[:, None]
    back_index = jnp.sum(
        jnp.where(hits, jnp.arange(slots_piece, dtype=jnp.int32)[None, :], 0), axis=1
    )
    expert_out = jnp.take(summed, back_index, axis=1).reshape(
        column_width, expert_devices, seat_count
    )
    returned = lax.all_to_all(expert_out, "ep", split_axis=1, concat_axis=1, tiled=True)
    token_range = jnp.arange(local_tokens, dtype=jnp.int32)
    combine = jnp.where(
        (source_index[None, :] == token_range[:, None]) & filled[None, :], seat_weight[None, :], 0.0
    )
    mixed_out = jnp.einsum(
        "tb,cb->tc",
        combine,
        returned.reshape(column_width, buffer_rows).astype(jnp.float32),
        precision=lax.Precision.HIGHEST,
    )
    return mixed_out.astype(jnp.bfloat16)


def solution(mesh):
    in_specs = (
        P("ep", None),
        P(),
        P(),
        P(),
        P(None, "ep", "tp"),
        P(None, "ep", "tp"),
        P(None, "ep", "tp"),
    )
    out_specs = P("ep", "tp")
    return jax.shard_map(body, mesh=mesh, in_specs=in_specs, out_specs=out_specs, check_vma=False)
```

profile of v0, /device:TPU:1, one launch (start us, length us, event | category | flops | bytes accessed | tf_op | source)
XLA Modules:
  0.0 247.3 jit_solution(16952757911391471088)
XLA Ops:
  0.0 2.1 broadcast_in_dim.134
  2.1 23.9 %all-to-all-start.1 = ((bf16[64,32,256]{2,1,0:T(8,128)(2,1)}), bf16[64,32,256]{2,1,0:T(8,128)(2,1)S(1)}, u32[]{:S(2)}, u32[]{:S(2)}) async-start(bf16[64,32,256]{2,1,0:T(8,128)(2,1)} %bitcast.10), calls=%async_computation.1 | async-start | bytes 2097152 | tf_op jit(solution)/shard_map/all_to_all | solution.py:59
  26.1 0.1 convert_reduce_fusion.1
  26.4 1.2 select_reduce_fusion.2
  27.6 25.9 %all-to-all-done.1 = bf16[64,32,256]{2,1,0:T(8,128)(2,1)S(1)} async-done(((bf16[64,32,256]{2,1,0:T(8,128)(2,1)}), bf16[64,32,256]{2,1,0:T(8,128)(2,1)S(1)}, u32[]{:S(2)}, u32[]{:S(2)}) %all-to-all-start.1) | async-done | bytes 1048608 | tf_op jit(solution)/shard_map/all_to_all | solution.py:59
  53.5 1.3 broadcast_in_dim.135
  54.8 8.0 %all-to-all-start.2 = ((bf16[64,32,256]{2,1,0:T(8,128)(2,1)}), bf16[64,32,256]{2,1,0:T(8,128)(2,1)}, u32[]{:S(2)}, u32[]{:S(2)}) async-start(bf16[64,32,256]{2,1,0:T(8,128)(2,1)} %bitcast.12), calls=%async_computation.2 | async-start | bytes 2097152 | tf_op jit(solution)/shard_map/all_to_all | solution.py:60
  62.9 0.2 fusion.3
  63.1 0.2 fusion.5
  63.3 2.5 gather_fusion
  65.8 1.2 fusion.7
  67.0 1.7 fusion
  68.6 20.4 %all-to-all-done.2 = bf16[64,32,256]{2,1,0:T(8,128)(2,1)} async-done(((bf16[64,32,256]{2,1,0:T(8,128)(2,1)}), bf16[64,32,256]{2,1,0:T(8,128)(2,1)}, u32[]{:S(2)}, u32[]{:S(2)}) %all-to-all-start.2) | async-done | bytes 1048608 | tf_op jit(solution)/shard_map/all_to_all | solution.py:60
  89.0 57.2 %all_to_all.42 = bf16[64,8,2048]{2,1,0:T(8,128)(2,1)S(1)} all-to-all(bf16[64,8,2048]{2,1,0:T(8,128)(2,1)} %fusion), channel_id=1, replica_groups=mesh['ep'=64,'tp'=16] {'ep'}, dimensions={0} | all-to-all | bytes 4194304 | tf_op jit(solution)/shard_map/all_to_all | solution.py:65
  146.3 1.2 broadcast_in_dim.136
  147.4 8.7 %all-to-all-start.3 = ((bf16[64,32,256]{2,1,0:T(8,128)(2,1)}), bf16[64,32,256]{2,1,0:T(8,128)(2,1)}, u32[]{:S(2)}, u32[]{:S(2)}) async-start(bf16[64,32,256]{2,1,0:T(8,128)(2,1)} %bitcast.14), calls=%async_computation.3 | async-start | bytes 2097152 | tf_op jit(solution)/shard_map/all_to_all | solution.py:62
  156.1 0.2 convert_reduce_fusion
  156.4 1.4 gather_fusion.1
  157.7 1.7 fusion.8
  159.4 21.9 %all-to-all-done.3 = bf16[64,32,256]{2,1,0:T(8,128)(2,1)} async-done(((bf16[64,32,256]{2,1,0:T(8,128)(2,1)}), bf16[64,32,256]{2,1,0:T(8,128)(2,1)}, u32[]{:S(2)}, u32[]{:S(2)}) %all-to-all-start.3) | async-done | bytes 1048608 | tf_op jit(solution)/shard_map/all_to_all | solution.py:62
  181.3 2.9 %fusion.1 = bf16[32,16,8,128]{3,2,1,0:T(8,128)(2,1)S(1)} fusion(bf16[2048,256]{1,0:T(8,128)(2,1)} %bitcast.15, bf16[2048,256]{1,0:T(8,128)(2,1)} %bitcast.13, bf16[256,2048]{1,0:T(8,128)(2,1)S(1)} %gather_fusion.1, pred[256]{0:T(512)(128)(4,1)S(1)} %compare_and_fusion.2, f32[256,256]{1,0:T(8,128)S(1)} %fusion.8), kind=kOutput, calls=%fused_computation.6 | convolution fusion | flops 538312704 | bytes 4456704 | tf_op jit(solution)/shard_map/df,bf->db/dot_general | solution.py:78
  184.2 1.3 copy.12
  185.4 12.4 %all-to-all-start.4 = ((bf16[16,128,256]{1,2,0:T(8,128)(2,1)}), bf16[16,128,256]{1,2,0:T(8,128)(2,1)S(1)}, u32[]{:S(2)}, u32[]{:S(2)}) async-start(bf16[16,128,256]{1,2,0:T(8,128)(2,1)} %bitcast.45), calls=%async_computation.4 | async-start | bytes 2097152 | tf_op jit(solution)/shard_map/all_to_all | solution.py:16
  197.9 0.1 select_reduce_fusion
  198.2 27.7 %all-to-all-done.4 = bf16[16,128,256]{1,2,0:T(8,128)(2,1)S(1)} async-done(((bf16[16,128,256]{1,2,0:T(8,128)(2,1)}), bf16[16,128,256]{1,2,0:T(8,128)(2,1)S(1)}, u32[]{:S(2)}, u32[]{:S(2)}) %all-to-all-start.4) | async-done | bytes 1048608 | tf_op jit(solution)/shard_map/all_to_all | solution.py:16
  225.9 0.1 reduce_sum.83
  226.0 1.3 gather_fusion.2
  227.4 0.8 bitcast_select_fusion.1
  228.1 6.0 %all-to-all-start.5 = ((bf16[128,64,8]{0,2,1:T(8,128)(2,1)}), bf16[128,64,8]{0,2,1:T(8,128)(2,1)S(1)}, u32[]{:S(2)}, u32[]{:S(2)}) async-start(bf16[128,64,8]{0,2,1:T(8,128)(2,1)} %bitcast_select_fusion.1), calls=%async_computation.5 | async-start | bytes 262144 | tf_op jit(solution)/shard_map/all_to_all | solution.py:92
  234.4 0.2 select_reduce_fusion.1
  234.7 11.7 %all-to-all-done.5 = bf16[128,64,8]{0,2,1:T(8,128)(2,1)S(1)} async-done(((bf16[128,64,8]{0,2,1:T(8,128)(2,1)}), bf16[128,64,8]{0,2,1:T(8,128)(2,1)S(1)}, u32[]{:S(2)}, u32[]{:S(2)}) %all-to-all-start.5) | async-done | bytes 131104 | tf_op jit(solution)/shard_map/all_to_all | solution.py:92
  246.3 0.9 convolution_convert_fusion.1
  (36 shorter events, 0.8 us)
Async XLA Ops:
  0.0 26.0 %copy-start.4 = (s32[8,2048]{1,0:T(8,128)S(1)}, s32[8,2048]{1,0:T(8,128)}, u32[]{:S(2)}) copy-start(s32[8,2048]{1,0:T(8,128)} %param.9) | copy-start | bytes 196612
  0.0 53.5 %copy-start.2 = (bf16[8,32,256]{2,1,0:T(8,128)(2,1)S(1)}, bf16[8,32,256]{2,1,0:T(8,128)(2,1)}, u32[]{:S(2)}) copy-start(bf16[8,32,256]{2,1,0:T(8,128)(2,1)} %param.12) | copy-start | bytes 393220
  2.1 51.4 %all-to-all-start.1 = ((bf16[64,32,256]{2,1,0:T(8,128)(2,1)}), bf16[64,32,256]{2,1,0:T(8,128)(2,1)S(1)}, u32[]{:S(2)}, u32[]{:S(2)}) async-start(bf16[64,32,256]{2,1,0:T(8,128)(2,1)} %bitcast.10), calls=%async_computation.1 | async-start | bytes 2097152 | tf_op jit(solution)/shard_map/all_to_all | solution.py:59
  26.0 36.8 %copy-start = (bf16[128,2048]{1,0:T(8,128)(2,1)S(1)}, bf16[128,2048]{1,0:T(8,128)(2,1)}, u32[]{:S(2)}) copy-start(bf16[128,2048]{1,0:T(8,128)(2,1)} %param.7) | copy-start | bytes 1572868
  26.2 36.9 %copy-start.6 = (f32[2048]{0:T(1024)S(1)}, f32[2048]{0:T(1024)}, u32[]{:S(2)}) copy-start(f32[2048]{0:T(1024)} %param.8) | copy-start | bytes 24580
  53.5 9.6 %copy-start.1 = (bf16[64,32,256]{2,1,0:T(8,128)(2,1)}, bf16[64,32,256]{2,1,0:T(8,128)(2,1)S(1)}, u32[]{:S(2)}) copy-start(bf16[64,32,256]{2,1,0:T(8,128)(2,1)S(1)} %all-to-all-done.1) | copy-start | bytes 3145732
  54.8 34.2 %all-to-all-start.2 = ((bf16[64,32,256]{2,1,0:T(8,128)(2,1)}), bf16[64,32,256]{2,1,0:T(8,128)(2,1)}, u32[]{:S(2)}, u32[]{:S(2)}) async-start(bf16[64,32,256]{2,1,0:T(8,128)(2,1)} %bitcast.12), calls=%async_computation.2 | async-start | bytes 2097152 | tf_op jit(solution)/shard_map/all_to_all | solution.py:60
  68.6 77.6 %copy-start.3 = (bf16[8,32,256]{2,1,0:T(8,128)(2,1)S(1)}, bf16[8,32,256]{2,1,0:T(8,128)(2,1)}, u32[]{:S(2)}) copy-start(bf16[8,32,256]{2,1,0:T(8,128)(2,1)} %param.13) | copy-start | bytes 393220
  147.4 33.9 %all-to-all-start.3 = ((bf16[64,32,256]{2,1,0:T(8,128)(2,1)}), bf16[64,32,256]{2,1,0:T(8,128)(2,1)}, u32[]{:S(2)}, u32[]{:S(2)}) async-start(bf16[64,32,256]{2,1,0:T(8,128)(2,1)} %bitcast.14), calls=%async_computation.3 | async-start | bytes 2097152 | tf_op jit(solution)/shard_map/all_to_all | solution.py:62
  185.4 48.9 %copy-start.5 = (f32[8,2048]{1,0:T(8,128)S(1)}, f32[8,2048]{1,0:T(8,128)}, u32[]{:S(2)}) copy-start(f32[8,2048]{1,0:T(8,128)} %param.10) | copy-start | bytes 196612
  185.4 40.4 %all-to-all-start.4 = ((bf16[16,128,256]{1,2,0:T(8,128)(2,1)}), bf16[16,128,256]{1,2,0:T(8,128)(2,1)S(1)}, u32[]{:S(2)}, u32[]{:S(2)}) async-start(bf16[16,128,256]{1,2,0:T(8,128)(2,1)} %bitcast.45), calls=%async_computation.4 | async-start | bytes 2097152 | tf_op jit(solution)/shard_map/all_to_all | solution.py:16
  228.1 18.2 %all-to-all-start.5 = ((bf16[128,64,8]{0,2,1:T(8,128)(2,1)}), bf16[128,64,8]{0,2,1:T(8,128)(2,1)S(1)}, u32[]{:S(2)}, u32[]{:S(2)}) async-start(bf16[128,64,8]{0,2,1:T(8,128)(2,1)} %bitcast_select_fusion.1), calls=%async_computation.5 | async-start | bytes 262144 | tf_op jit(solution)/shard_map/all_to_all | solution.py:92
where the time goes:
time: 248 us; the launch traced here: 247 us
  waiting for transfers between devices  107 us (43%)
  starting transfers between devices  59.1 us (24%)
  blocking collectives  57.2 us (23%)
  local copies, waits for them, and re-layouts  11.4 us (5%)
  other arithmetic  6.26 us (3%)
  matrix products  5.48 us (2%)
    all_to_all x1, blocking collectives, body(): lax.all_to_all(outgoing.reshape(expert_devices, seat_count, model_width),...  57.2 us
    all_to_all x1, waiting for transfers between devices, sum_at_owner(): lax.all_to_all(tiles, axis, split_axis=0, concat_axis=0, tiled=True)  27.7 us
    all_to_all x1, waiting for transfers between devices, body(): lax.all_to_all(gate_send, 'ep', split_axis=0, concat_axis=1, tiled=True)  25.9 us
    all_to_all x1, starting transfers between devices, body(): lax.all_to_all(gate_send, 'ep', split_axis=0, concat_axis=1, tiled=True)  23.9 us
    all_to_all x1, waiting for transfers between devices, body(): lax.all_to_all(down_send, 'ep', split_axis=0, concat_axis=1, tiled=True)  21.9 us
    all_to_all x1, waiting for transfers between devices, body(): lax.all_to_all(up_send, 'ep', split_axis=0, concat_axis=1, tiled=True)  20.4 us
    all_to_all x1, starting transfers between devices, sum_at_owner(): lax.all_to_all(tiles, axis, split_axis=0, concat_axis=0, tiled=True)  12.4 us
    all_to_all x1, waiting for transfers between devices, body(): lax.all_to_all(expert_out, 'ep', split_axis=1, concat_axis=1, tiled=True)  11.7 us
  transfers between devices with their start and end apart: 5, of which 5 were waited for; matrix products, arithmetic and copies ran while one was open for 5% of the time, Pallas kernels for 0%

commit v1 on v0

v1 whole, which is shorter than its diff:
```python
import jax
import jax.numpy as jnp
from jax import lax
from jax.experimental import pallas as pl
from jax.experimental.pallas import tpu as pltpu
from jax.sharding import PartitionSpec as P

EPSILON = 1e-06
N = 8
TOK = 128
SEATS = 8
SLOTS = 256
ROWS = N * N * SEATS
F32, BF16 = jnp.float32, jnp.bfloat16


def dot(a, b, ca, cb):
    return lax.dot_general(a, b, (((ca,), (cb,)), ((), ())), preferred_element_type=F32)


def kernel(
    tokens, gain, chosen, slotw, wg, wu, wd, out,
    W, OH, OHR, WS, OUT, B, A, X, HID, ACC, QS, Q, S, T, R, U, V,
    z_s, z_r, ring_s, ring_r, ry_s, ry_r, rz_s, rz_r, xg_s, xg_r, dg_s, dg_r,
    q_s, q_r, t_s, t_r, u_s, u_r, v_s, v_r,
):
    me = lax.axis_index("ep")
    tp = lax.axis_index("tp")
    z, y = me // N, me % N
    x, c = tp // 2, tp % 2
    weights = (wg, wu, wd)

    def z_peer(d):
        return {"ep": (z + d) % N * N + y}

    def y_peer(d):
        return {"ep": z * N + (y + d) % N}

    def x_peer(d):
        return {"tp": (x + d) % N * 2 + c}

    partner = {"tp": x * 2 + 1 - c}

    def remote(src, dst, send, recv, device):
        return pltpu.make_async_remote_copy(
            src_ref=src, dst_ref=dst, send_sem=send, recv_sem=recv, device_id=device,
            device_id_type=pl.DeviceIdType.MESH,
        )

    def each(count, body):
        def step(i, carry):
            body(i)
            return carry

        lax.fori_loop(0, count, step, 0)

    barrier = pltpu.get_barrier_semaphore()

    def greet(i):
        for peer in (z_peer, y_peer, x_peer):
            pl.semaphore_signal(barrier, inc=1, device_id=peer(i + 1), device_id_type=pl.DeviceIdType.MESH)

    each(N - 1, greet)
    pl.semaphore_signal(barrier, inc=1, device_id=partner, device_id_type=pl.DeviceIdType.MESH)

    for k in range(3):
        W[k, z, y] = weights[k][z]

    tok = chosen[...]
    local = (tok - me * TOK).astype(F32)
    mine = (local >= 0) & (local < TOK)
    first = jnp.sum(jnp.where(local < 0, 1.0, 0.0), axis=1, keepdims=True)
    slot_range = lax.broadcasted_iota(jnp.int32, (N * N, SLOTS), 1).astype(F32)
    key = jnp.where(mine, slot_range - first, -1.0)
    seat = lax.broadcasted_iota(jnp.int32, (N * N, SEATS, SLOTS), 1).astype(F32)
    match = key[:, None, :] == seat
    found = jnp.sum(jnp.where(match, local[:, None, :] + 1.0, 0.0), axis=2, keepdims=True)
    weight = jnp.sum(jnp.where(match, slotw[...][:, None, :], 0.0), axis=2, keepdims=True)
    found = found.reshape(ROWS, 1)
    token_range = lax.broadcasted_iota(jnp.int32, (ROWS, TOK), 1).astype(F32) + 1.0
    pick = jnp.where(found == token_range, 1.0, 0.0).astype(BF16)
    OH[...] = pick
    WS[...] = jnp.broadcast_to(weight.reshape(ROWS, 1), (ROWS, 128))

    values = tokens[...].astype(F32)
    scale = lax.rsqrt(jnp.mean(values * values, axis=1, keepdims=True) + EPSILON)
    columns = pl.ds(pl.multiple_of(tp * 128, 128), 128)
    normed = (tokens[:, columns].astype(F32) * scale * gain[pl.ds(tp, 1), :]).astype(BF16)
    OUT[...] = dot(pick, normed, 1, 0).reshape(N, N, SEATS, 128).astype(BF16)

    owner = (chosen[pl.ds(me, 1), :] // TOK).astype(F32)
    owner_range = lax.broadcasted_iota(jnp.int32, (N * N, SLOTS), 0).astype(F32)
    below = jnp.sum(jnp.where(owner < owner_range, 1.0, 0.0), axis=1, keepdims=True)
    count = jnp.sum(jnp.where(owner == owner_range, 1.0, 0.0), axis=1, keepdims=True)
    seat_of = slot_range - below
    seat_of = jnp.where((seat_of >= 0) & (seat_of < count), seat_of, -1.0)
    OHR[...] = jnp.where(seat_of[:, None, :] == seat, 1.0, 0.0).reshape(ROWS, SLOTS).astype(BF16)

    pl.semaphore_wait(barrier, 3 * (N - 1) + 1)

    def ry(d):
        return remote(OUT.at[:, (y + d) % N], B.at[y], ry_s.at[d - 1], ry_r.at[d - 1], y_peer(d))

    def ry_in(d):
        return remote(OUT.at[:, y], B.at[(y - d) % N], ry_s.at[d - 1], ry_r.at[d - 1], y_peer(d))

    each(N - 1, lambda i: ry(i + 1).start())
    B[y] = OUT[:, y]

    def send_z(k):
        each(
            N - 1,
            lambda i: remote(
                weights[k].at[(z + i + 1) % N], W.at[k, z, y], z_s.at[k, i], z_r.at[k, i], z_peer(i + 1)
            ).start(),
        )

    def wait_z(k, half):
        for i in range(N // 2):
            source = half * (N // 2) + i

            @pl.when(source != z)
            def _():
                d = (z - source) % N
                remote(
                    W.at[k, source, y], W.at[k, source, y], z_s.at[k, d - 1], z_r.at[k, d - 1], z_peer(d)
                ).wait_recv()

    def hops(way, half):
        return 4 if way == half else 3

    def ring(k, half, way, hop):
        sign = 1 - 2 * way
        block = W.at[k, pl.ds(half * 4, 4), (y - sign * hop) % N]
        chunk = k * 2 + half
        return remote(block, block, ring_s.at[way, chunk, hop], ring_r.at[way, chunk, hop], y_peer(sign))

    def ring_in(k, half, way, hop):
        sign = 1 - 2 * way
        block = W.at[k, pl.ds(half * 4, 4), (y - sign * (hop + 1)) % N]
        chunk = k * 2 + half
        return remote(block, block, ring_s.at[way, chunk, hop], ring_r.at[way, chunk, hop], y_peer(sign))

    def ring_hop(kinds, hop):
        for k in kinds:
            for half in range(2):
                if hop == 0:
                    wait_z(k, half)
                for way in range(2):
                    if 0 < hop <= hops(way, half):
                        ring_in(k, half, way, hop - 1).wait_recv()
                    if hop < hops(way, half):
                        ring(k, half, way, hop).start()

    send_z(0)
    send_z(1)

    each(N - 1, lambda i: ry_in(i + 1).wait_recv())

    def rz(d):
        return remote(B.at[:, (z + d) % N], A.at[z], rz_s.at[d - 1], rz_r.at[d - 1], z_peer(d))

    def rz_in(d):
        return remote(B.at[:, z], A.at[(z - d) % N], rz_s.at[d - 1], rz_r.at[d - 1], z_peer(d))

    each(N - 1, lambda i: rz(i + 1).start())
    A[z] = B[:, z]
    send_z(2)

    ring_hop((0, 1), 0)

    each(N - 1, lambda i: rz_in(i + 1).wait_recv())
    arrived = A[...].astype(F32).reshape(ROWS, 128).astype(BF16)
    own_columns = pl.ds(pl.multiple_of(c * 128, 128), 128)
    X[x, :, own_columns] = dot(OHR[...], arrived, 0, 0).astype(BF16)

    def xg(d):
        block = X.at[x, :, own_columns]
        return remote(block, block, xg_s.at[d - 1], xg_r.at[d - 1], x_peer(d))

    def xg_in(d):
        block = X.at[(x - d) % N, :, own_columns]
        return remote(block, block, xg_s.at[d - 1], xg_r.at[d - 1], x_peer(d))

    def dg(d):
        block = X.at[(x - d) % N, :, own_columns]
        return remote(block, block, dg_s.at[d], dg_r.at[d], partner)

    def dg_in(d):
        block = X.at[(x - d) % N, :, pl.ds(pl.multiple_of((1 - c) * 128, 128), 128)]
        return remote(block, block, dg_s.at[d], dg_r.at[d], partner)

    for d in (4, 3, 5, 2, 6, 1, 7):
        xg(d).start()
    dg(0).start()

    ring_hop((0, 1), 1)
    ring_hop((0, 1), 2)
    for d in (1, 7, 2, 6, 3, 5, 4):
        xg_in(d).wait_recv()
        dg(d).start()
    ring_hop((0, 1), 3)
    ring_hop((2,), 0)
    ring_hop((0, 1), 4)
    each(N, lambda d: dg_in(d).wait_recv())

    gate = jnp.zeros((SLOTS, 256), F32)
    up = jnp.zeros((SLOTS, 256), F32)
    for block in range(N):
        rows = X[block]
        gate += dot(rows, W[0, block].reshape(256, 256), 1, 0)
        up += dot(rows, W[1, block].reshape(256, 256), 1, 0)
    HID[...] = (gate / (1.0 + jnp.exp(-gate)) * up).astype(BF16)

    def q_copy(j):
        return remote(QS.at[j], Q.at[j], q_s.at[j], q_r.at[j], partner)

    def t_copy(j, d):
        return remote(S.at[j, (x + d) % N], T.at[x, j], t_s.at[j, d - 1], t_r.at[j, d - 1], x_peer(d))

    def t_in(j, d):
        return remote(S.at[j, x], T.at[(x - d) % N, j], t_s.at[j, d - 1], t_r.at[j, d - 1], x_peer(d))

    def share(b):
        part = dot(W[2, :, b].reshape(256, 256), HID[...], 1, 1)
        j = b % 4

        @pl.when(b // 4 == c)
        def _():
            ACC[j] = part

        @pl.when(b // 4 != c)
        def _():
            QS[j] = part.astype(BF16)
            q_copy(j).start()

    def spread(b):
        j = b % 4

        @pl.when(b // 4 == c)
        def _():
            q_copy(j).wait_recv()
            S[j] = (ACC[j] + Q[j].astype(F32)).reshape(N, 32, SLOTS).astype(BF16)
            T[x, j] = S[j, x]
            for d in (4, 3, 5, 2, 6, 1, 7):
                t_copy(j, d).start()

    share(y)
    for hop in range(1, 5):
        ring_hop((2,), hop)
        if hop < 4:
            share((y - hop) % N)
            spread((y + hop - 1) % N)
            share((y + hop) % N)
            spread((y - hop) % N)
        else:
            share((y + 4) % N)
            spread((y + 3) % N)
            spread((y + 4) % N)

    each(4, lambda j: each(N - 1, lambda i: t_in(j, i + 1).wait_recv()))
    total = T[0].astype(F32)
    for source in range(1, N):
        total += T[source].astype(F32)
    total = total.reshape(128, SLOTS).astype(BF16)

    R[...] = dot(OHR[...], total, 1, 1).reshape(N, N, SEATS, 128).astype(BF16)

    def back_z(d):
        return remote(R.at[(z + d) % N], U.at[z], u_s.at[d - 1], u_r.at[d - 1], z_peer(d))

    def back_z_in(d):
        return remote(R.at[z], U.at[(z - d) % N], u_s.at[d - 1], u_r.at[d - 1], z_peer(d))

    def back_y(d):
        return remote(U.at[:, (y + d) % N], V.at[:, y], v_s.at[d - 1], v_r.at[d - 1], y_peer(d))

    def back_y_in(d):
        return remote(U.at[:, y], V.at[:, (y - d) % N], v_s.at[d - 1], v_r.at[d - 1], y_peer(d))

    each(N - 1, lambda i: back_z(i + 1).start())
    U[z] = R[z]
    each(N - 1, lambda i: back_z_in(i + 1).wait_recv())
    each(N - 1, lambda i: back_y(i + 1).start())
    V[:, y] = U[:, y]
    each(N - 1, lambda i: back_y_in(i + 1).wait_recv())

    weighted = V[...].astype(F32).reshape(ROWS, 128) * WS[...]
    high = weighted.astype(BF16)
    low = (weighted - high.astype(F32)).astype(BF16)
    out[...] = (dot(OH[...], high, 0, 0) + dot(OH[...], low, 0, 0)).astype(BF16)

    def z_sent(i):
        for k in range(3):
            remote(W.at[k, z, y], W.at[k, z, y], z_s.at[k, i], z_r.at[k, i], z_peer(i + 1)).wait_send()
        ry(i + 1).wait_send()
        rz(i + 1).wait_send()
        xg(i + 1).wait_send()
        for j in range(4):
            t_copy(j, i + 1).wait_send()
        back_z(i + 1).wait_send()
        back_y(i + 1).wait_send()

    each(N - 1, z_sent)
    each(N, lambda d: dg(d).wait_send())
    each(4, lambda j: q_copy(j).wait_send())

    def ring_sent(k):
        for half in range(2):
            for way in range(2):
                for hop in range(hops(way, half)):
                    ring(k, half, way, hop).wait_send()

    each(3, ring_sent)


def body(tokens, norm_gain, chosen, slot_weight, gate_weight, up_weight, down_weight):
    dma = pltpu.SemaphoreType.DMA
    vmem = pl.BlockSpec(memory_space=pltpu.VMEM)
    seats = (N, N, SEATS, 128)

    def pair(*shape):
        return [dma(shape), dma(shape)]

    return pl.pallas_call(
        kernel,
        out_shape=jax.ShapeDtypeStruct((TOK, 128), BF16),
        in_specs=[vmem] * 7,
        out_specs=vmem,
        scratch_shapes=[
            pltpu.VMEM((3, N, N, 32, 256), BF16),
            pltpu.VMEM((ROWS, TOK), BF16),
            pltpu.VMEM((ROWS, SLOTS), BF16),
            pltpu.VMEM((ROWS, 128), F32),
            pltpu.VMEM(seats, BF16),
            pltpu.VMEM(seats, BF16),
            pltpu.VMEM(seats, BF16),
            pltpu.VMEM((N, SLOTS, 256), BF16),
            pltpu.VMEM((SLOTS, 256), BF16),
            pltpu.VMEM((4, 256, SLOTS), F32),
            pltpu.VMEM((4, 256, SLOTS), BF16),
            pltpu.VMEM((4, 256, SLOTS), BF16),
            pltpu.VMEM((4, N, 32, SLOTS), BF16),
            pltpu.VMEM((N, 4, 32, SLOTS), BF16),
            pltpu.VMEM(seats, BF16),
            pltpu.VMEM(seats, BF16),
            pltpu.VMEM(seats, BF16),
            *pair(3, N - 1),
            *pair(2, 6, 4),
            *pair(N - 1),
            *pair(N - 1),
            *pair(N - 1),
            *pair(N),
            *pair(4),
            *pair(4, N - 1),
            *pair(N - 1),
            *pair(N - 1),
        ],
        compiler_params=pltpu.CompilerParams(
            collective_id=0, has_side_effects=True, vmem_limit_bytes=40 * 1024 * 1024
        ),
    )(
        tokens,
        norm_gain.reshape(16, 128),
        chosen.reshape(N * N, SLOTS),
        slot_weight.reshape(N * N, SLOTS),
        gate_weight,
        up_weight,
        down_weight,
    )


def solution(mesh):
    in_specs = (
        P("ep", None),
        P(),
        P(),
        P(),
        P(None, "ep", "tp"),
        P(None, "ep", "tp"),
        P(None, "ep", "tp"),
    )
    return jax.shard_map(body, mesh=mesh, in_specs=in_specs, out_specs=P("ep", "tp"), check_vma=False)
```

time: 248 us -> 91.2 us (0.37)
  waiting for transfers between devices: 107 us -> 0 us
  Pallas kernels: 0 us -> 84.7 us
  starting transfers between devices: 59.1 us -> 0 us
  blocking collectives: 57.2 us -> 0 us
  local copies, waits for them, and re-layouts: 11.4 us -> 5.02 us
  other arithmetic: 6.26 us -> 0 us
  matrix products: 5.48 us -> 0 us
    all_to_all x5 -> x0, waiting for transfers between devices: 107 us -> none  [the longest x1 27.7 us: sum_at_owner(): lax.all_to_all(tiles, axis, split_axis=0, concat_axis=0, tiled=True)]
    pallas_call x0 -> x1, Pallas kernels: none -> 84.7 us  [body(): pl.pallas_call(kernel, out_shape=jax.ShapeDtypeStruct((TOK, 128), BF16),...]
    all_to_all x5 -> x0, starting transfers between devices: 59.1 us -> none  [the longest x1 23.9 us: body(): lax.all_to_all(gate_send, 'ep', split_axis=0, concat_axis=1, tiled=True)]
    all_to_all x1 -> x0, blocking collectives: 57.2 us -> none  [body(): lax.all_to_all(outgoing.reshape(expert_devices, seat_count, model_width),...]
    dot_general x3 -> x0, matrix products: 5.48 us -> none  [the longest x1 2.86 us: body(): jnp.einsum('df,bf->db', down_rows, hidden, preferred_element_type=jnp.flo...]
    gather x3 -> x0, local copies, waits for them, and re-layouts: 5.17 us -> none  [the longest x1 2.47 us: body(): jnp.take(normed, source_index, axis=0)]
    broadcast_in_dim x5 -> x0, local copies, waits for them, and re-layouts: 4.61 us -> none  [the longest x1 2.06 us: body(): gate_send = jnp.repeat(gate_weight, group_size, axis=0)]
    unnamed x14 -> x11, local copies, waits for them, and re-layouts: 0.03 us -> 3.26 us
  transfers between devices with their start and end apart: 5 -> 0, of which waited for: 5 -> 0; matrix products, arithmetic and copies ran while one was open for 5% -> 0% of each run, Pallas kernels for 0% -> 0%
where the time goes in v1:
time: 91.2 us; the launch traced here: 89.8 us
  Pallas kernels  84.7 us (93%)
  local copies, waits for them, and re-layouts  5.02 us (6%)
    pallas_call x1, Pallas kernels, body(): pl.pallas_call(kernel, out_shape=jax.ShapeDtypeStruct((TOK, 128), BF16),...  84.7 us
    unnamed x11, local copies, waits for them, and re-layouts  3.26 us

profile of v1, /device:TPU:1, one launch (start us, length us, event | category | flops | bytes accessed | tf_op | source)
XLA Modules:
  0.0 89.8 jit_solution(8453222478600095930)
XLA Ops:
  0.0 0.0 copy-start.1
  0.0 0.0 copy-start.2
  0.0 0.9 %reshape.10.chosen = s32[64,256]{1,0:T(8,128)S(1)} reshape(s32[8,2048]{1,0:T(8,128)} %param.9) | data formatting | bytes 131072 | tf_op jit(solution)/shard_map/reshape | solution.py:365
  0.9 0.9 reshape.11.slotw
  1.8 0.0 copy-done.1
  1.8 0.0 copy-done.2
  1.8 0.0 copy-start
  1.8 1.0 %copy-done = bf16[128,2048]{1,0:T(8,128)(2,1)S(1)} copy-done((bf16[128,2048]{1,0:T(8,128)(2,1)S(1)}, bf16[128,2048]{1,0:T(8,128)(2,1)}, u32[]{:S(2)}) %copy-start) | copy-done | bytes 524312
  2.8 0.0 copy-start.3
  2.8 0.9 %copy-done.3 = bf16[8,32,256]{2,1,0:T(8,128)(2,1)S(1)} copy-done((bf16[8,32,256]{2,1,0:T(8,128)(2,1)S(1)}, bf16[8,32,256]{2,1,0:T(8,128)(2,1)}, u32[]{:S(2)}) %copy-start.3) | copy-done | bytes 131096
  3.7 0.0 copy-start.4
  3.7 0.7 copy-done.4
  4.4 84.7 %shard_map.73 = bf16[128,128]{1,0:T(8,128)(2,1)S(1)} custom-call(bf16[128,2048]{1,0:T(8,128)(2,1)S(1)} %copy-done, f32[16,128]{1,0:T(8,128)S(1)} %bitcast.1, s32[64,256]{1,0:T(8,128)S(1)} %reshape.10.chosen, f32[64,256]{1,0:T(8,128)S(1)} %reshape.11.slotw, bf16[8,32,256]{2,1,0:T(8,128)(2,1)S(1)} %copy-done.1, bf16[8,32,256]{2,1,0:T(8,128)(2,1)S(1)} %copy-done.2, ...), custom_call_target="tpu_custom_call" | custom-call | tf_op jit(solution)/shard_map/pallas_call | solution.py:325
  89.1 0.6 copy.9
Async XLA Ops:
  0.0 1.8 %copy-start.1 = (bf16[8,32,256]{2,1,0:T(8,128)(2,1)S(1)}, bf16[8,32,256]{2,1,0:T(8,128)(2,1)}, u32[]{:S(2)}) copy-start(bf16[8,32,256]{2,1,0:T(8,128)(2,1)} %wg.1) | copy-start | bytes 393220
  0.0 1.8 %copy-start.2 = (bf16[8,32,256]{2,1,0:T(8,128)(2,1)S(1)}, bf16[8,32,256]{2,1,0:T(8,128)(2,1)}, u32[]{:S(2)}) copy-start(bf16[8,32,256]{2,1,0:T(8,128)(2,1)} %wu.1) | copy-start | bytes 393220
  1.8 1.0 %copy-start = (bf16[128,2048]{1,0:T(8,128)(2,1)S(1)}, bf16[128,2048]{1,0:T(8,128)(2,1)}, u32[]{:S(2)}) copy-start(bf16[128,2048]{1,0:T(8,128)(2,1)} %tokens.1) | copy-start | bytes 1572868
  2.8 0.9 %copy-start.3 = (bf16[8,32,256]{2,1,0:T(8,128)(2,1)S(1)}, bf16[8,32,256]{2,1,0:T(8,128)(2,1)}, u32[]{:S(2)}) copy-start(bf16[8,32,256]{2,1,0:T(8,128)(2,1)} %wd.1) | copy-start | bytes 393220
  3.7 0.7 copy-start.4

commit v2 on v1

v2 whole, which is shorter than its diff:
```python
import jax
import jax.numpy as jnp
from jax import lax
from jax.experimental import pallas as pl
from jax.experimental.pallas import tpu as pltpu
from jax.sharding import PartitionSpec as P

EPSILON = 1e-06
N = 8
TOK = 128
SEATS = 8
SLOTS = 256
ROWS = N * N * SEATS
F32, BF16 = jnp.float32, jnp.bfloat16


def dot(a, b, ca, cb):
    return lax.dot_general(a, b, (((ca,), (cb,)), ((), ())), preferred_element_type=F32)


NEAR = (0, 1, 7, 2, 6, 3, 5, 4)
FAR = (4, 3, 5, 2, 6, 1, 7)


def kernel(
    tokens, gain, chosen, slotw, wg, wu, wd, out,
    TK, GN, CH, SW, SGU, SD, WGU, WD, OH, OHR, WS, OUT, B, B2, A, X, HID, ACC, QS, Q, S, T, R, U, U2, V,
    in_sem, z_s, z_r, zd_s, zd_r, g_s, g_r, d_s, d_r, ry_s, ry_r, rz_s, rz_r, xg_s, xg_r, dg_s, dg_r,
    q_s, q_r, t_s, t_r, u_s, u_r, v_s, v_r,
):
    me = lax.axis_index("ep")
    tp = lax.axis_index("tp")
    z, y = me // N, me % N
    x, c = tp // 2, tp % 2

    def z_peer(d):
        return {"ep": (z + d) % N * N + y}

    def y_peer(d):
        return {"ep": z * N + (y + d) % N}

    def x_peer(d):
        return {"tp": (x + d) % N * 2 + c}

    partner = {"tp": x * 2 + 1 - c}

    def remote(src, dst, send, recv, device):
        return pltpu.make_async_remote_copy(
            src_ref=src, dst_ref=dst, send_sem=send, recv_sem=recv, device_id=device,
            device_id_type=pl.DeviceIdType.MESH,
        )

    def each(count, body):
        def step(i, carry):
            body(i)
            return carry

        lax.fori_loop(0, count, step, 0)

    fetches = [
        pltpu.make_async_copy(source, target, in_sem.at[i])
        for i, (source, target) in enumerate(
            (
                (chosen, CH), (tokens, TK), (slotw, SW), (gain, GN),
                (wg, SGU.at[:, 0]), (wu, SGU.at[:, 1]),
                (wg.at[z], WGU.at[z, y, 0]), (wu.at[z], WGU.at[z, y, 1]),
                (wd, SD), (wd.at[z], WD.at[y, z]),
            )
        )
    ]
    for fetch in fetches:
        fetch.start()

    barrier = pltpu.get_barrier_semaphore()

    def greet(i):
        for peer in (z_peer, y_peer, x_peer):
            pl.semaphore_signal(barrier, inc=1, device_id=peer(i + 1), device_id_type=pl.DeviceIdType.MESH)

    each(N - 1, greet)
    pl.semaphore_signal(barrier, inc=1, device_id=partner, device_id_type=pl.DeviceIdType.MESH)
    for fetch in fetches:
        fetch.wait()

    def pieces(ref):
        return jnp.concatenate([ref[:, i * SLOTS : (i + 1) * SLOTS] for i in range(N)], axis=0)

    local = (pieces(CH) - me * TOK).astype(F32)
    mine = (local >= 0) & (local < TOK)
    first = jnp.sum(jnp.where(local < 0, 1.0, 0.0), axis=1, keepdims=True)
    slot_range = lax.broadcasted_iota(jnp.int32, (N * N, SLOTS), 1).astype(F32)
    key = jnp.where(mine, slot_range - first, -1.0)
    seat = lax.broadcasted_iota(jnp.int32, (N * N, SEATS, SLOTS), 1).astype(F32)
    match = key[:, None, :] == seat
    found = jnp.sum(jnp.where(match, local[:, None, :] + 1.0, 0.0), axis=2, keepdims=True)
    weight = jnp.sum(jnp.where(match, pieces(SW)[:, None, :], 0.0), axis=2, keepdims=True)
    found = found.reshape(ROWS, 1)
    token_range = lax.broadcasted_iota(jnp.int32, (ROWS, TOK), 1).astype(F32) + 1.0
    pick = jnp.where(found == token_range, 1.0, 0.0).astype(BF16)
    OH[...] = pick
    WS[...] = jnp.broadcast_to(weight.reshape(ROWS, 1), (ROWS, 128))

    values = TK[...].astype(F32)
    scale = lax.rsqrt(jnp.mean(values * values, axis=1, keepdims=True) + EPSILON)
    columns = pl.ds(pl.multiple_of(tp * 128, 128), 128)
    normed = (TK[:, columns].astype(F32) * scale * GN[pl.ds(tp, 1), :]).astype(BF16)
    OUT[...] = dot(pick, normed, 1, 0).reshape(N, N, SEATS, 128).astype(BF16)

    owner = (CH[pl.ds(z, 1), pl.ds(pl.multiple_of(y * SLOTS, SLOTS), SLOTS)] // TOK).astype(F32)
    owner_range = lax.broadcasted_iota(jnp.int32, (N * N, SLOTS), 0).astype(F32)
    below = jnp.sum(jnp.where(owner < owner_range, 1.0, 0.0), axis=1, keepdims=True)
    count = jnp.sum(jnp.where(owner == owner_range, 1.0, 0.0), axis=1, keepdims=True)
    seat_of = slot_range - below
    seat_of = jnp.where((seat_of >= 0) & (seat_of < count), seat_of, -1.0)
    OHR[...] = jnp.where(seat_of[:, None, :] == seat, 1.0, 0.0).reshape(ROWS, SLOTS).astype(BF16)

    pl.semaphore_wait(barrier, 3 * (N - 1) + 1)

    def ry(d):
        return remote(OUT.at[(y + d) % N], B.at[y], ry_s.at[d - 1], ry_r.at[d - 1], y_peer(d))

    def ry_in(d):
        return remote(OUT.at[y], B.at[(y - d) % N], ry_s.at[d - 1], ry_r.at[d - 1], y_peer(d))

    def rz(d):
        return remote(B2.at[(z + d) % N], A.at[z], rz_s.at[d - 1], rz_r.at[d - 1], z_peer(d))

    def rz_in(d):
        return remote(B2.at[z], A.at[(z - d) % N], rz_s.at[d - 1], rz_r.at[d - 1], z_peer(d))

    def zgu(d):
        return remote(SGU.at[(z + d) % N], WGU.at[z, y], z_s.at[d - 1], z_r.at[d - 1], z_peer(d))

    def zgu_in(d):
        return remote(SGU.at[z], WGU.at[(z - d) % N, y], z_s.at[d - 1], z_r.at[d - 1], z_peer(d))

    def zd(d):
        return remote(SD.at[(z + d) % N], WD.at[y, z], zd_s.at[d - 1], zd_r.at[d - 1], z_peer(d))

    def zd_in(d):
        return remote(SD.at[z], WD.at[y, (z - d) % N], zd_s.at[d - 1], zd_r.at[d - 1], z_peer(d))

    def hops(way, chunk):
        return 4 if way == chunk % 2 else 3

    def gu(chunk, way, hop, come):
        sign = 1 - 2 * way
        block = WGU.at[(z + NEAR[chunk]) % N, (y - sign * (hop + come)) % N]
        return remote(block, block, g_s.at[way, chunk, hop], g_r.at[way, chunk, hop], y_peer(sign))

    def down(chunk, way, hop, come):
        sign = 1 - 2 * way
        block = WD.at[(y - sign * (hop + come)) % N, pl.ds(chunk * 2, 2)]
        return remote(block, block, d_s.at[way, chunk, hop], d_r.at[way, chunk, hop], y_peer(sign))

    def ring(copy, chunk, hop):
        for way in range(2):
            if 0 < hop <= hops(way, chunk):
                copy(chunk, way, hop - 1, 1).wait_recv()
            if hop < hops(way, chunk):
                copy(chunk, way, hop, 0).start()

    def gu_first(chunk):
        if chunk > 0:
            zgu_in((N - NEAR[chunk]) % N).wait_recv()
        ring(gu, chunk, 0)

    each(N - 1, lambda i: ry(i + 1).start())
    for d in NEAR[1:]:
        zgu(d).start()
    B[y] = OUT[y]
    for chunk in range(5):
        gu_first(chunk)

    each(N - 1, lambda i: ry_in(i + 1).wait_recv())
    for i in range(N):
        B2[i] = B[:, i]
    each(N - 1, lambda i: rz(i + 1).start())
    for d in NEAR[1:]:
        zd(d).start()
    A[z] = B2[z]

    ring(gu, 0, 1)
    gu_first(5)
    gu_first(6)
    ring(gu, 1, 1)
    gu_first(7)
    for chunk in (2, 3, 4):
        ring(gu, chunk, 1)

    each(N - 1, lambda i: rz_in(i + 1).wait_recv())
    arrived = A[...].astype(F32).reshape(ROWS, 128).astype(BF16)
    own_columns = pl.ds(pl.multiple_of(c * 128, 128), 128)
    X[x, :, own_columns] = dot(OHR[...], arrived, 0, 0).astype(BF16)

    def xg(d):
        block = X.at[x, :, own_columns]
        return remote(block, block, xg_s.at[d - 1], xg_r.at[d - 1], x_peer(d))

    def xg_in(d):
        block = X.at[(x - d) % N, :, own_columns]
        return remote(block, block, xg_s.at[d - 1], xg_r.at[d - 1], x_peer(d))

    def dg(d):
        block = X.at[(x - d) % N, :, own_columns]
        return remote(block, block, dg_s.at[d], dg_r.at[d], partner)

    def dg_in(d):
        block = X.at[(x - d) % N, :, pl.ds(pl.multiple_of((1 - c) * 128, 128), 128)]
        return remote(block, block, dg_s.at[d], dg_r.at[d], partner)

    for d in FAR:
        xg(d).start()
    dg(0).start()

    for chunk in (5, 6, 7):
        ring(gu, chunk, 1)
    for hop in (2, 3):
        for chunk in range(8):
            ring(gu, chunk, hop)
    each(N - 1, lambda i: zd_in(i + 1).wait_recv())
    for chunk in range(4):
        ring(down, chunk, 0)
    for d in (1, 7, 2, 6, 3, 5, 4):
        xg_in(d).wait_recv()
        dg(d).start()
    for chunk in range(8):
        ring(gu, chunk, 4)
    each(N, lambda d: dg_in(d).wait_recv())

    gate = jnp.zeros((SLOTS, 256), F32)
    up = jnp.zeros((SLOTS, 256), F32)
    for block in range(N):
        rows = X[block]
        gate += dot(rows, WGU[block, :, 0].reshape(256, 256), 1, 0)
        up += dot(rows, WGU[block, :, 1].reshape(256, 256), 1, 0)
    HID[...] = (gate / (1.0 + jnp.exp(-gate)) * up).astype(BF16)

    def q_copy(j):
        return remote(QS.at[j], Q.at[j], q_s.at[j], q_r.at[j], partner)

    def t_copy(j, d):
        return remote(S.at[j, (x + d) % N], T.at[x, j], t_s.at[j, d - 1], t_r.at[j, d - 1], x_peer(d))

    def t_in(j, d):
        return remote(S.at[j, x], T.at[(x - d) % N, j], t_s.at[j, d - 1], t_r.at[j, d - 1], x_peer(d))

    def share(b):
        part = dot(WD[b].reshape(256, 256), HID[...], 1, 1)
        j = b % 4

        @pl.when(b // 4 == c)
        def _():
            ACC[j] = part

        @pl.when(b // 4 != c)
        def _():
            QS[j] = part.astype(BF16)
            q_copy(j).start()

    def spread(b):
        j = b % 4

        @pl.when(b // 4 == c)
        def _():
            q_copy(j).wait_recv()
            S[j] = (ACC[j] + Q[j].astype(F32)).reshape(N, 32, SLOTS).astype(BF16)
            T[x, j] = S[j, x]
            for d in FAR:
                t_copy(j, d).start()

    share(y)
    for hop in range(1, 5):
        for chunk in range(4):
            ring(down, chunk, hop)
        if hop < 4:
            share((y - hop) % N)
            spread((y + hop - 1) % N)
            share((y + hop) % N)
            spread((y - hop) % N)
        else:
            share((y + 4) % N)
            spread((y + 3) % N)
            spread((y + 4) % N)

    each(4, lambda j: each(N - 1, lambda i: t_in(j, i + 1).wait_recv()))
    total = T[0].astype(F32)
    for source in range(1, N):
        total += T[source].astype(F32)
    total = total.reshape(128, SLOTS).astype(BF16)

    R[...] = dot(OHR[...], total, 1, 1).reshape(N, N, SEATS, 128).astype(BF16)

    def back_z(d):
        return remote(R.at[(z + d) % N], U.at[z], u_s.at[d - 1], u_r.at[d - 1], z_peer(d))

    def back_z_in(d):
        return remote(R.at[z], U.at[(z - d) % N], u_s.at[d - 1], u_r.at[d - 1], z_peer(d))

    def back_y(d):
        return remote(U2.at[(y + d) % N], V.at[y], v_s.at[d - 1], v_r.at[d - 1], y_peer(d))

    def back_y_in(d):
        return remote(U2.at[y], V.at[(y - d) % N], v_s.at[d - 1], v_r.at[d - 1], y_peer(d))

    for d in FAR:
        back_z(d).start()
    U[z] = R[z]
    each(N - 1, lambda i: back_z_in(i + 1).wait_recv())
    for i in range(N):
        U2[i] = U[:, i]
    for d in FAR:
        back_y(d).start()
    V[y] = U2[y]
    each(N - 1, lambda i: back_y_in(i + 1).wait_recv())

    weighted = V[...].astype(F32).reshape(ROWS, 128) * WS[...]
    high = weighted.astype(BF16)
    low = (weighted - high.astype(F32)).astype(BF16)
    out[...] = (dot(OH[...], high, 0, 0) + dot(OH[...], low, 0, 0)).astype(BF16)

    def sent(i):
        for copy in (ry, rz, zgu, zd, xg, back_z, back_y):
            copy(i + 1).wait_send()
        for j in range(4):
            t_copy(j, i + 1).wait_send()

    each(N - 1, sent)
    each(N, lambda d: dg(d).wait_send())
    each(4, lambda j: q_copy(j).wait_send())
    for copy, count in ((gu, 8), (down, 4)):
        for chunk in range(count):
            for way in range(2):
                for hop in range(hops(way, chunk)):
                    copy(chunk, way, hop, 0).wait_send()


def body(tokens, norm_gain, chosen, slot_weight, gate_weight, up_weight, down_weight):
    dma = pltpu.SemaphoreType.DMA
    seats = pltpu.VMEM((N, N, SEATS, 128), BF16)

    def pair(*shape):
        return [dma(shape), dma(shape)]

    return pl.pallas_call(
        kernel,
        out_shape=jax.ShapeDtypeStruct((TOK, 128), BF16),
        in_specs=[pl.BlockSpec(memory_space=pl.ANY)] * 7,
        out_specs=pl.BlockSpec(memory_space=pltpu.VMEM),
        scratch_shapes=[
            pltpu.VMEM((TOK, 2048), BF16),
            pltpu.VMEM((16, 128), F32),
            pltpu.VMEM((N, N * SLOTS), jnp.int32),
            pltpu.VMEM((N, N * SLOTS), F32),
            pltpu.VMEM((N, 2, 32, 256), BF16),
            pltpu.VMEM((N, 32, 256), BF16),
            pltpu.VMEM((N, N, 2, 32, 256), BF16),
            pltpu.VMEM((N, N, 32, 256), BF16),
            pltpu.VMEM((ROWS, TOK), BF16),
            pltpu.VMEM((ROWS, SLOTS), BF16),
            pltpu.VMEM((ROWS, 128), F32),
            *[seats] * 4,
            pltpu.VMEM((N, SLOTS, 256), BF16),
            pltpu.VMEM((SLOTS, 256), BF16),
            pltpu.VMEM((4, 256, SLOTS), F32),
            pltpu.VMEM((4, 256, SLOTS), BF16),
            pltpu.VMEM((4, 256, SLOTS), BF16),
            pltpu.VMEM((4, N, 32, SLOTS), BF16),
            pltpu.VMEM((N, 4, 32, SLOTS), BF16),
            *[seats] * 4,
            dma((10,)),
            *pair(N - 1),
            *pair(N - 1),
            *pair(2, 8, 4),
            *pair(2, 4, 4),
            *pair(N - 1),
            *pair(N - 1),
            *pair(N - 1),
            *pair(N),
            *pair(4),
            *pair(4, N - 1),
            *pair(N - 1),
            *pair(N - 1),
        ],
        compiler_params=pltpu.CompilerParams(
            collective_id=0, has_side_effects=True, vmem_limit_bytes=60 * 1024 * 1024
        ),
    )(tokens, norm_gain.reshape(16, 128), chosen, slot_weight, gate_weight, up_weight, down_weight)


def solution(mesh):
    in_specs = (
        P("ep", None),
        P(),
        P(),
        P(),
        P(None, "ep", "tp"),
        P(None, "ep", "tp"),
        P(None, "ep", "tp"),
    )
    return jax.shard_map(body, mesh=mesh, in_specs=in_specs, out_specs=P("ep", "tp"), check_vma=False)
```

time: 91.2 us -> 85.6 us (0.939)
  the two profiles are of different devices: /device:TPU:1 before, /device:TPU:16 now
where the time goes in v2:
time: 85.6 us; the launch traced here: 85.4 us
  Pallas kernels  84 us (98%)
  local copies, waits for them, and re-layouts  1.38 us (2%)
    pallas_call x1, Pallas kernels, body(): pl.pallas_call(kernel, out_shape=jax.ShapeDtypeStruct((TOK, 128), BF16),...  84 us

profile of v2, /device:TPU:16, one launch (start us, length us, event | category | flops | bytes accessed | tf_op | source)
XLA Modules:
  0.0 85.4 jit_solution(337035685646770889)
XLA Ops:
  0.0 84.0 %shard_map.73 = bf16[128,128]{1,0:T(8,128)(2,1)} custom-call(bf16[128,2048]{1,0:T(8,128)(2,1)} %tokens.1, f32[16,128]{1,0:T(8,128)} %bitcast.1, s32[8,2048]{1,0:T(8,128)} %chosen.1, f32[8,2048]{1,0:T(8,128)} %slotw.1, bf16[8,32,256]{2,1,0:T(8,128)(2,1)} %wg.1, bf16[8,32,256]{2,1,0:T(8,128)(2,1)} %wu.1, bf16[8,32,256]{2,1,0:T(8,128)(2,1)} %wd.1), custom_call_target="tpu_custom_call" | custom-call | tf_op jit(solution)/shard_map/pallas_call | solution.py:345
  84.0 1.4 %copy.9 = bf16[128,128]{1,0:T(8,128)(2,1)} copy(bf16[128,128]{1,0:T(8,128)(2,1)} %shard_map.73) | data formatting | bytes 65536
